TPU v7x, 256 devices: a 8x8x2 block of a 8x8x16 slice. The times are simulated.
256 devices in a mesh: grp: 2 (over z), ep: 16 (over y, core), tp: 8 (over x).
Axes of the slice: x: 8, y: 8, z: 2, core: 2. Of those that a mesh axis runs over, the one named last changes fastest.
The devices are a block of a 8x8x16 slice.
Arguments:
- tokens: bfloat16 [8192, 4096], P(('grp', 'ep')), parts along dimension 0, may hold values from -6 to 6
- expert_ids: int32 [8192, 2], P(('grp', 'ep')), parts along dimension 0, may hold values from 0 to 15, as said below
- gates: float32 [8192, 2], P(('grp', 'ep')), parts along dimension 0, may hold values from 0.1 to 1
- w_gate: bfloat16 [16, 4096, 2048], P('ep', None, 'tp'), may hold values from -0.09375 to 0.09375
- w_up: bfloat16 [16, 4096, 2048], P('ep', None, 'tp'), may hold values from -0.09375 to 0.09375
- w_down: bfloat16 [16, 2048, 4096], P('ep', 'tp'), may hold values from -0.79549513 to 0.79549513, as said below
- norm_gain: float32 [4096], P('tp'), may hold values from 0.1 to 1.9
- norm_bias: float32 [4096], P('tp'), may hold values from -1.5 to 1.5
Outputs:
- normed: bfloat16 [8192, 4096], P(('grp', 'ep'), 'tp'), parts along dimension 0
There are 2 independent parts, one for each index of `grp`. A program takes and returns all parts, laid end to end along the dimension named above; an argument that names none is the same for every part. Nothing has to cross between parts.
Inputs may be any that keep to these rules, and one draw needn't show every extreme that they name: `expert_ids`: each row names 2 different experts, both in the same group of 4 consecutive expert numbers. Within one aligned block of 256 rows no expert is named more than 64 times, and in every draw some expert is named exactly 64 times in every block. `w_down`: down projection weights.
All inputs are finite; a program needn't handle non-finite values.
Results may differ from a plain program's by a relative error of at most 0.014.
Values may be sent and summed in bfloat16 or wider, within the bound.
A program may use at most 128 MiB of HBM per device.

v0:
```python
import jax
import jax.numpy as jnp
from jax import lax
from jax.sharding import PartitionSpec as P

D = 4096
TOPK = 2
EXPERTS = 16
CAP = 64


norm_eps = 1e-05


def copy_for_each(value, axis):
    peers = lax.axis_size(axis)
    return lax.all_to_all(
        jnp.broadcast_to(value[None], (peers, *value.shape)), axis, 0, 0, tiled=True
    )


def of_everyone(value, axis):
    everything = copy_for_each(value, axis)
    return jnp.sum(everything, axis=0)


def together(arrays, axis):
    ends = [0]
    for a in arrays:
        ends.append(ends[-1] + a.size)
    subtotal = of_everyone(jnp.concatenate([a.ravel() for a in arrays]), axis)
    return tuple((subtotal[b:e].reshape(a.shape) for a, b, e in zip(arrays, ends, ends[1:])))


def route_slots(expert_ids):
    flat_ids = expert_ids.reshape(-1)
    onehot = (flat_ids[:, None] == jnp.arange(EXPERTS, dtype=jnp.int32)[None, :]).astype(jnp.int32)
    position = jnp.sum((jnp.cumsum(onehot, axis=0) - 1) * onehot, axis=1)
    target = flat_ids * CAP + position
    token_of = jnp.arange(flat_ids.shape[0], dtype=jnp.int32) // TOPK
    source = jnp.zeros((EXPERTS * CAP,), jnp.int32).at[target].set(token_of)
    filled = jnp.zeros((EXPERTS * CAP,), jnp.bool_).at[target].set(True)
    return (target, source, filled)


def on_device(tokens, expert_ids, gates, w_gate, w_up, w_down, norm_gain, norm_bias):
    tok_rows, width = tokens.shape
    piece_width = norm_gain.shape[0]
    target, source, filled = route_slots(expert_ids)
    offset = lax.axis_index("tp") * piece_width
    own_columns = lax.dynamic_slice_in_dim(tokens, offset, piece_width, 1)
    outgoing = jnp.where(filled[:, None], own_columns[source], jnp.zeros((), jnp.bfloat16)).reshape(
        EXPERTS, CAP, piece_width
    )
    arrived = lax.all_to_all(outgoing, "ep", split_axis=0, concat_axis=1, tiled=True)
    segment = lax.all_gather(arrived, "tp", axis=2, tiled=True)
    gate_more = jnp.einsum("erd,edf->erf", segment, w_gate, preferred_element_type=jnp.float32)
    up_more = jnp.einsum("erd,edf->erf", segment, w_up, preferred_element_type=jnp.float32)
    hidden = (jax.nn.silu(gate_more) * up_more).astype(jnp.bfloat16)
    partial_value = jnp.einsum("erf,efd->erd", hidden, w_down, preferred_element_type=jnp.float32)
    summed = lax.psum_scatter(
        partial_value.astype(jnp.bfloat16), "tp", scatter_dimension=2, tiled=True
    )
    returned = lax.all_to_all(summed, "ep", split_axis=1, concat_axis=0, tiled=True)
    picked = returned.reshape(EXPERTS * CAP, piece_width)[target].reshape(
        tok_rows, TOPK, piece_width
    )
    combined = jnp.sum(picked.astype(jnp.float32) * gates[:, :, None], axis=1)
    stats = together((jnp.sum(combined, axis=1), jnp.sum(combined * combined, axis=1)), "tp")
    row_mean = stats[0] / D
    row_var = stats[1] / D - row_mean * row_mean
    normed = (combined - row_mean[:, None]) * lax.rsqrt(
        row_var[:, None] + norm_eps
    ) * norm_gain + norm_bias
    return normed.astype(jnp.bfloat16)


def solution(mesh):
    return jax.shard_map(
        on_device,
        mesh=mesh,
        in_specs=(
            P(("grp", "ep"), None),
            P(("grp", "ep"), None),
            P(("grp", "ep"), None),
            P("ep", None, "tp"),
            P("ep", None, "tp"),
            P("ep", "tp", None),
            P("tp"),
            P("tp"),
        ),
        out_specs=P(("grp", "ep"), "tp"),
        check_vma=False,
    )
```

profile of v0, /device:TPU:513, one launch (start us, length us, event | category | flops | bytes accessed | tf_op | source)
XLA Modules:
  0.0 358.6 jit_solution(16169199813096574413)
XLA Ops:
  6.5 0.0 copy-start
  6.6 0.0 all-gather.2.cloned.1.call-start
  6.6 1.0 copy.38
  7.5 0.1 eq.29
  7.7 0.1 eq.25
  7.8 0.7 broadcast_multiply_fusion
  8.5 1.2 reduce-window.6
  9.7 0.2 slice_reduce_fusion
  9.9 0.1 copy.37
  10.1 0.1 mul.70
  10.2 0.1 fusion.18
  10.3 2.4 scatter_custom_fusion.1
  12.8 2.4 scatter_custom_fusion
  15.3 0.1 broadcast_in_dim.24
  15.3 1.0 constant_dynamic-slice_fusion
  16.3 4.0 %gather_fusion = bf16[1024,512]{1,0:T(8,128)(2,1)S(1)} fusion(bf16[256,512]{1,0:T(8,128)(2,1)S(1)} %constant_dynamic-slice_fusion, s32[1024]{0:T(1024)S(1)} %fusion.20), kind=kCustom, calls=%fused_computation | custom fusion | bytes 2101248 | tf_op jit(solution)/shard_map/gather | solution.py:52
  20.3 0.2 broadcast_select_fusion
  20.5 52.0 %all_to_all.27 = bf16[16,64,512]{2,1,0:T(8,128)(2,1)} all-to-all(bf16[16,64,512]{2,1,0:T(8,128)(2,1)S(1)} %broadcast_select_fusion), channel_id=1, replica_groups=mesh['grp'=2,'ep'=16,'tp'=8] {'ep'}, dimensions={0} | all-to-all | bytes 2097152 | tf_op jit(solution)/shard_map/all_to_all | solution.py:55
  72.5 0.1 all-gather.2.cloned.1.call-update
  72.5 0.2 reduce-scatter.2.cloned.1.call-start
  72.8 92.8 %all-gather.2.cloned.1.call-done = bf16[1,1024,4096]{2,1,0:T(8,128)(2,1)} async-done(((bf16[1,1024,512]{2,1,0:T(8,128)(2,1)}), bf16[1,1024,4096]{2,1,0:T(8,128)(2,1)}) %all-gather.2.cloned.1.call-update) | async-done | bytes 8388624 | tf_op jit(solution)/shard_map/all_gather | solution.py:56
  165.6 0.0 copy-start.5
  165.6 0.0 copy-start.6
  165.6 6.5 %fusion.2 = f32[1024,256]{1,0:T(8,128)S(1)} fusion(bf16[1,1024,4096]{2,1,0:T(8,128)(2,1)} %all-gather.2.cloned.1.call-done, bf16[1,4096,256]{2,1,0:T(8,128)(2,1)} %param.11), kind=kOutput, calls=%fused_computation.6 | convolution fusion | flops 2147483648 | bytes 11534336 | tf_op jit(solution)/shard_map/erd,edf->erf/dot_general | solution.py:57
  172.1 0.0 copy-done.5
  172.1 0.5 copy-done.6
  172.6 2.4 fusion.12
  174.9 0.0 copy-done
  174.9 5.6 %convert_bitcast_fusion = bf16[1,1024,4096]{2,1,0:T(8,128)(2,1)} fusion(bf16[1024,256]{1,0:T(8,128)(2,1)S(1)} %fusion.12, bf16[1,256,4096]{2,1,0:T(8,128)(2,1)S(1)} %copy-done), kind=kOutput, calls=%fused_computation.8 | convolution fusion | flops 2151677952 | bytes 11010048 | tf_op jit(solution)/shard_map/erf,efd->erd/dot_general | solution.py:60
  180.5 0.1 reduce-scatter.2.cloned.1.call-update
  180.6 95.3 %reduce-scatter.2.cloned.1.call-done = bf16[1,1024,512]{2,1,0:T(8,128)(2,1)} async-done(((bf16[1,1024,4096]{2,1,0:T(8,128)(2,1)}), bf16[1,1024,512]{2,1,0:T(8,128)(2,1)}) %reduce-scatter.2.cloned.1.call-update) | async-done | bytes 1048592 | tf_op jit(solution)/shard_map/reduce_scatter | solution.py:61
  275.8 4.2 %copy.54 = bf16[1,1024,512]{2,0,1:T(2,128)(2,1)} copy(bf16[1,1024,512]{2,1,0:T(8,128)(2,1)} %reduce-scatter.2.cloned.1.call-done) | data formatting | bytes 2097152 | tf_op jit(solution)/shard_map/reduce_scatter | solution.py:61
  280.0 0.5 broadcast.121
  280.5 8.3 %reduce.6 = bf16[1024,512]{1,0:T(8,128)(2,1)S(1)} reduce(bf16[1024,1,512]{2,1,0:T(2,128)(2,1)} %bitcast.53, bf16[]{:T(256)} %broadcast.121), dimensions={1}, to_apply=%bitcast.50.reduce_sub_computation | reduce | bytes 2097154
  288.8 0.0 copy-start.2
  288.8 1.6 reshape.155
  290.4 7.7 %all-to-all-start.1 = ((bf16[16,2,16384]{2,1,0:T(2,128)(2,1)}), bf16[16,2,16384]{2,1,0:T(2,128)(2,1)S(1)}, u32[]{:S(2)}, u32[]{:S(2)}) async-start(bf16[16,2,16384]{2,1,0:T(2,128)(2,1)} %reshape.155), calls=%async_computation.2 | async-start | bytes 2097152 | tf_op jit(solution)/shard_map/all_to_all | solution.py:64
  298.1 0.0 copy-done.2
  298.1 0.1 copy.42
  298.3 0.1 mul.77
  298.4 27.7 %all-to-all-done.1 = bf16[16,2,16384]{2,1,0:T(2,128)(2,1)S(1)} async-done(((bf16[16,2,16384]{2,1,0:T(2,128)(2,1)}), bf16[16,2,16384]{2,1,0:T(2,128)(2,1)S(1)}, u32[]{:S(2)}, u32[]{:S(2)}) %all-to-all-start.1) | async-done | bytes 1048608 | tf_op jit(solution)/shard_map/all_to_all | solution.py:64
  326.1 3.5 reshape.156
  329.6 1.9 copy.53
  331.4 2.6 gather_fusion.1
  334.1 0.0 copy-start.1
  334.1 0.0 copy-start.3
  334.1 0.0 copy-start.4
  334.1 2.8 reshape.116
  336.8 2.6 multiply_reduce_fusion.1
  339.4 0.1 multiply_reduce_fusion.2
  339.6 0.0 copy-done.1
  339.6 0.3 multiply_reduce_fusion
  339.8 0.1 reduce_sum.58
  340.0 0.1 reduce_sum.59
  340.1 10.7 %all_to_all.28 = f32[8,1,512]{2,1,0:T(1,128)S(1)} all-to-all(f32[8,1,512]{2,1,0:T(1,128)S(1)} %broadcast_in_dim.45), channel_id=1, replica_groups=mesh['grp'=2,'ep'=16,'tp'=8] {'tp'}, dimensions={0} | all-to-all | bytes 32768 | tf_op jit(solution)/shard_map/all_to_all | solution.py:17
  350.8 0.0 copy-done.3
  350.9 0.0 copy-done.4
  350.9 0.9 add_convert_fusion
  (12 shorter events, 0.1 us)
Async XLA Ops:
  6.5 168.4 %copy-start = (bf16[1,256,4096]{2,1,0:T(8,128)(2,1)S(1)}, bf16[1,256,4096]{2,1,0:T(8,128)(2,1)}, u32[]{:S(2)}) copy-start(bf16[1,256,4096]{2,1,0:T(8,128)(2,1)} %param.13) | copy-start | bytes 6291460
  6.6 159.0 %all-gather.2.cloned.1.call-start = ((), (), s32[]{:S(2)}) async-start(), calls=%async_computation.4 | async-start | bytes 9437184 | tf_op jit(solution)/shard_map/all_gather | solution.py:56
  72.5 203.3 %reduce-scatter.2.cloned.1.call-start = ((), (), s32[]{:S(2)}) async-start(), calls=%async_computation.5 | async-start | bytes 9437184 | tf_op jit(solution)/shard_map/reduce_scatter | solution.py:61
  165.6 6.5 %copy-start.5 = (bf16[1,1024,4096]{2,1,0:T(8,128)(2,1)S(1)}, bf16[1,1024,4096]{2,1,0:T(8,128)(2,1)}, u32[]{:S(2)}) copy-start(bf16[1,1024,4096]{2,1,0:T(8,128)(2,1)} %all-gather.2.cloned.1.call-done) | copy-start | bytes 25165828
  165.6 7.0 %copy-start.6 = (bf16[1,4096,256]{2,1,0:T(8,128)(2,1)S(1)}, bf16[1,4096,256]{2,1,0:T(8,128)(2,1)}, u32[]{:S(2)}) copy-start(bf16[1,4096,256]{2,1,0:T(8,128)(2,1)} %param.12) | copy-start | bytes 6291460
  288.8 9.3 %copy-start.2 = (f32[256,2]{0,1:T(2,128)S(1)}, f32[256,2]{0,1:T(2,128)}, u32[]{:S(2)}) copy-start(f32[256,2]{0,1:T(2,128)} %param.10) | copy-start | bytes 6148
  290.4 35.7 %all-to-all-start.1 = ((bf16[16,2,16384]{2,1,0:T(2,128)(2,1)}), bf16[16,2,16384]{2,1,0:T(2,128)(2,1)S(1)}, u32[]{:S(2)}, u32[]{:S(2)}) async-start(bf16[16,2,16384]{2,1,0:T(2,128)(2,1)} %reshape.155), calls=%async_computation.2 | async-start | bytes 2097152 | tf_op jit(solution)/shard_map/all_to_all | solution.py:64
  334.1 5.5 %copy-start.1 = (bf16[512,512]{1,0:T(8,128)(2,1)S(1)}, bf16[512,512]{1,0:T(8,128)(2,1)}, u32[]{:S(2)}) copy-start(bf16[512,512]{1,0:T(8,128)(2,1)} %gather_fusion.1) | copy-start | bytes 1572868
  334.1 16.8 %copy-start.3 = (f32[512]{0:T(512)S(1)}, f32[512]{0:T(512)}, u32[]{:S(2)}) copy-start(f32[512]{0:T(512)} %param.15) | copy-start | bytes 6148
  334.1 16.8 %copy-start.4 = (f32[512]{0:T(512)S(1)}, f32[512]{0:T(512)}, u32[]{:S(2)}) copy-start(f32[512]{0:T(512)} %param.14) | copy-start | bytes 6148
Sparse Core Ops, SparseCore 0:
  72.7 92.8 all-gather.1
  180.7 95.0 reduce-scatter.1
where the time goes:
time: 359 us
  waiting for transfers between devices  216 us (60%)
  blocking collectives  62.7 us (17%)
  local copies, waits for them, and re-layouts  29.6 us (8%)
  other arithmetic  14.4 us (4%)
  matrix products  14.4 us (4%)
  between operations  13.7 us (4%)
  starting transfers between devices  7.98 us (2%)
    reduce_scatter x1, waiting for transfers between devices, on_device(): lax.psum_scatter(partial_value.astype(jnp.bfloat16), 'tp', scatter_dimens...  95.3 us
    all_gather x1, waiting for transfers between devices, on_device(): segment = lax.all_gather(arrived, 'tp', axis=2, tiled=True)  92.8 us
    all_to_all x1, blocking collectives, on_device(): lax.all_to_all(outgoing, 'ep', split_axis=0, concat_axis=1, tiled=True)  52 us
    all_to_all x1, waiting for transfers between devices, on_device(): lax.all_to_all(summed, 'ep', split_axis=1, concat_axis=0, tiled=True)  27.7 us
    all_to_all x1, blocking collectives, copy_for_each(): lax.all_to_all(jnp.broadcast_to(value[None], (peers, *value.shape)), axis...  10.7 us
    unnamed x20, local copies, waits for them, and re-layouts  9.03 us
    unnamed x1, other arithmetic  8.25 us
    all_to_all x1, starting transfers between devices, on_device(): lax.all_to_all(summed, 'ep', split_axis=1, concat_axis=0, tiled=True)  7.73 us
  transfers between devices with their start and end apart: 3, of which 3 were waited for; matrix products, arithmetic and copies ran while one was open for 0% of the time, Pallas kernels for 0%

commit v1 on v0

v1 whole, which is shorter than its diff:
```python
import functools

import jax
import jax.numpy as jnp
from jax import lax
from jax.experimental import pallas as pl
from jax.experimental.pallas import tpu as pltpu
from jax.sharding import PartitionSpec as P

CAP = 64
CORES = 2
EPS = 1e-05
BF = jnp.bfloat16
F32 = jnp.float32


def dot(a, b):
    return jnp.dot(a, b, preferred_element_type=F32)


def offset_of(i):
    half = (i + 1) // 2
    return half * (2 * lax.rem(i, 2) - 1)


def kernel(
    n_ep, n_tp, n_grp,
    tok_hbm, ids_ref, gates_ref, wg_hbm, wu_hbm, wd_hbm, gain_ref, bias_ref,
    out_ref,
    tok, wg, wu, wdc, routed, sendb, sib, hid, outb, ret, slots, stat,
    load_sem,
    ys_sem, yr_sem, xs_sem, xr_sem, hs_sem, hr_sem, rs_sem, rr_sem,
    ws_sem, wr_sem, zs_sem, zr_sem, ss_sem, sr_sem,
):
    n_y = n_ep // CORES
    tokens, width = tok.shape
    quarter = width // 4
    cols = width // n_tp
    ff = wg.shape[1]
    rows = CORES * CAP
    far = n_tp // 2
    me_g, me_e, me_x = (lax.axis_index(a) for a in ("grp", "ep", "tp"))
    me_y, me_c = me_e // CORES, lax.rem(me_e, CORES)
    half = lax.rem(me_x, 2)
    right, left = lax.rem(me_x + 1, n_tp), lax.rem(me_x + n_tp - 1, n_tp)
    mate = me_g + 1 - 2 * lax.rem(me_g, 2)
    wpart = lax.rem(me_g, 2)

    def x_at(s):
        return lax.rem(me_x + s + n_tp, n_tp)

    def chip_at(i):
        return lax.rem(me_y + offset_of(i) + n_y, n_y)

    def chunk_rows(chip):
        return pl.ds(pl.multiple_of(chip * rows, rows), rows)

    def block_rows(block):
        return pl.ds(pl.multiple_of(block * CAP, CAP), CAP)

    load_tok = pltpu.make_async_copy(tok_hbm, tok, load_sem.at[0])
    load_wg = pltpu.make_async_copy(wg_hbm, wg, load_sem.at[1])
    load_wu = pltpu.make_async_copy(wu_hbm, wu, load_sem.at[2])
    own_cols = pl.ds(pl.multiple_of(me_x * cols, cols), cols)
    own_w = pl.ds(pl.multiple_of(me_x * ff, ff), ff)
    load_wd = pltpu.make_async_copy(wd_hbm.at[:, own_cols], wdc.at[own_w], load_sem.at[3])
    load_tok.start()
    load_wg.start()
    load_wu.start()
    load_wd.start()

    barrier = pltpu.get_barrier_semaphore()
    for s in range(1, n_ep):
        pl.semaphore_signal(barrier, 1, device_id={"ep": lax.rem(me_e + s, n_ep)})
    for s in range(1, n_tp):
        pl.semaphore_signal(barrier, 1, device_id={"tp": lax.rem(me_x + s, n_tp)})
    pl.semaphore_signal(barrier, 1, device_id={"grp": mate})

    ids = ids_ref[...]
    lane = lax.broadcasted_iota(jnp.int32, (tokens, 128), 1)
    hit0 = lane == ids[:, 0:1]
    hit1 = lane == ids[:, 1:2]
    named = jnp.where(hit0 | hit1, 1.0, 0.0).astype(BF)
    t_row = lax.broadcasted_iota(jnp.int32, (tokens, tokens), 0)
    t_col = lax.broadcasted_iota(jnp.int32, (tokens, tokens), 1)
    before = jnp.where(t_col < t_row, 1.0, 0.0).astype(BF)
    position = dot(before, named)
    slot = position + (lane * CAP).astype(F32)
    slot0 = jnp.sum(jnp.where(hit0, slot, 0.0), axis=1, keepdims=True)
    slot1 = jnp.sum(jnp.where(hit1, slot, 0.0), axis=1, keepdims=True)
    slots[...] = jnp.where(lane == 0, slot0, jnp.where(lane == 1, slot1, -1.0)).T[:8]

    pl.semaphore_wait(barrier, n_ep - 1 + n_tp - 1 + 1)

    wrows = ff // 2

    def w_half(x, part):
        return pl.ds(pl.multiple_of(x * ff + part * wrows, wrows), wrows)

    def w_copy(i):
        x = x_at(offset_of(i + 1))
        return pltpu.make_async_remote_copy(
            wd_hbm.at[
                pl.ds(pl.multiple_of(wpart * wrows, wrows), wrows),
                pl.ds(pl.multiple_of(x * cols, cols), cols),
            ],
            wdc.at[w_half(me_x, wpart)],
            ws_sem.at[x], wr_sem.at[me_x], device_id={"tp": x},
        )

    def w_arrival(x):
        here = wdc.at[w_half(x, wpart)]
        return pltpu.make_async_remote_copy(
            here, here, ws_sem.at[x], wr_sem.at[x], device_id={"tp": x})

    def z_copy(x, part):
        here = wdc.at[w_half(x, part)]
        return pltpu.make_async_remote_copy(
            here, here, zs_sem.at[x], zr_sem.at[x], device_id={"grp": mate})

    @pl.loop(0, n_tp - 1)
    def _(i):
        w_copy(i).start()

    load_tok.wait()

    def spread(chip, column):
        s_iota = (chip * rows).astype(F32) + lax.broadcasted_iota(
            jnp.int32, (rows, tokens), 0).astype(F32)
        chosen = (s_iota == slots[0:1, :]) | (s_iota == slots[1:2, :])
        pick = jnp.where(chosen, 1.0, 0.0).astype(BF)
        return dot(pick, tok[:, pl.ds(pl.multiple_of(column, quarter), quarter)]).astype(BF)

    def y_copy(chip, core):
        expert = chip * CORES + core
        return pltpu.make_async_remote_copy(
            sendb.at[:, block_rows(expert)],
            routed.at[pl.ds(2 * half, 2), block_rows(me_e)],
            ys_sem.at[expert], yr_sem.at[me_e], device_id={"ep": expert},
        )

    def y_arrival(block):
        here = routed.at[pl.ds(2 * half, 2), block_rows(block)]
        return pltpu.make_async_remote_copy(
            here, here, ys_sem.at[block], yr_sem.at[block], device_id={"ep": block})

    sibling = me_y * CORES + 1 - me_c

    def sib_copy():
        return pltpu.make_async_remote_copy(
            sib, routed.at[:, block_rows(me_e)],
            ys_sem.at[sibling], yr_sem.at[me_e], device_id={"ep": sibling},
        )

    def sib_arrival():
        here = routed.at[:, block_rows(sibling)]
        return pltpu.make_async_remote_copy(
            here, here, ys_sem.at[sibling], yr_sem.at[sibling], device_id={"ep": sibling})

    @pl.loop(1, n_y)
    def _(i):
        chip = chip_at(i)
        for q in range(2):
            sendb[q, chunk_rows(chip), :] = spread(chip, (2 * half + q) * quarter)
        for core in range(CORES):
            y_copy(chip, core).start()

    @pl.loop(0, 4)
    def _(q):
        both = spread(me_y, q * quarter)
        swap = me_c == 0
        routed[q, block_rows(me_e), :] = jnp.where(swap, both[:CAP], both[CAP:])
        sib[q] = jnp.where(swap, both[CAP:], both[:CAP])

    sib_copy().start()

    def x_copy(chip, side):
        here = routed.at[2 * half + side, chunk_rows(chip)]
        return pltpu.make_async_remote_copy(
            here, here, xs_sem.at[side, chip], xr_sem.at[side, chip],
            device_id={"tp": (right, left)[side]})

    def x_arrival(chip, side):
        here = routed.at[2 * (1 - half) + side, chunk_rows(chip)]
        return pltpu.make_async_remote_copy(
            here, here, xs_sem.at[side, chip], xr_sem.at[side, chip],
            device_id={"tp": (left, right)[side]})

    def hid_part(chip, x, step, side):
        if step < far:
            return hid.at[x, chunk_rows(chip)]
        first = pl.multiple_of(chip * rows + side * CAP, CAP)
        return hid.at[x, pl.ds(first, rows // 2)]

    def hid_copy(chip, step, side):
        x = x_at((1 - step, step - 1)[side])
        here = hid_part(chip, x, step, side)
        return pltpu.make_async_remote_copy(
            here, here, hs_sem.at[side, step - 1, chip], hr_sem.at[side, step - 1, chip],
            device_id={"tp": (right, left)[side]})

    def hid_arrival(chip, step, side):
        x = x_at((-step, step)[side])
        here = hid_part(chip, x, step, side)
        return pltpu.make_async_remote_copy(
            here, here, hs_sem.at[side, step - 1, chip], hr_sem.at[side, step - 1, chip],
            device_id={"tp": (left, right)[side]})

    def ret_copy(chip, core):
        block = chip * CORES + core
        return pltpu.make_async_remote_copy(
            outb.at[block_rows(block)], ret.at[block_rows(me_e)],
            rs_sem.at[block], rr_sem.at[me_e], device_id={"ep": block})

    def ret_arrival(expert):
        here = ret.at[block_rows(expert)]
        return pltpu.make_async_remote_copy(
            here, here, rs_sem.at[expert], rr_sem.at[expert], device_id={"ep": expert})

    def forward(chip):
        for core in range(CORES):
            y_arrival(chip * CORES + core).wait_recv()
        for side in range(2):
            x_copy(chip, side).start()

    def first_layers(chip):
        here = chunk_rows(chip)
        gate = jnp.zeros((rows, ff), F32)
        up = jnp.zeros((rows, ff), F32)
        for q in range(4):
            part = routed[q, here, :]
            at = slice(q * quarter, (q + 1) * quarter)
            gate += dot(part, wg[at, :])
            up += dot(part, wu[at, :])
        hid[me_x, here, :] = (gate / (1.0 + jnp.exp(-gate)) * up).astype(BF)
        for side in range(2):
            hid_copy(chip, 1, side).start()

    def relay(chip, step):
        for side in range(2):
            hid_arrival(chip, step, side).wait_recv()
            hid_copy(chip, step + 1, side).start()

    def last_layer(chip):
        for side in range(2):
            hid_arrival(chip, far, side).wait_recv()
        here = chunk_rows(chip)
        acc = jnp.zeros((rows, cols), F32)
        for j in range(n_tp):
            acc += dot(hid[j, here, :], wdc[j * ff:(j + 1) * ff, :])
        outb[here, :] = acc.astype(BF)

    stages = far + 2
    lag_last = stages - 1

    @pl.loop(0, n_y + lag_last)
    def _(t):
        c = t - lag_last

        @pl.when(c == 0)
        def _():
            @pl.loop(1, n_tp)
            def _(s):
                z_copy(x_at(s), 1 - wpart).wait_recv()
            load_wd.wait()

        @pl.when((c >= 0) & (c < n_y))
        def _():
            chip = chip_at(c)
            last_layer(chip)

            @pl.when(c == 0)
            def _():
                ret[block_rows(me_e), :] = outb[block_rows(me_e), :]
                ret_copy(me_y, 1 - me_c).start()

            @pl.when(c > 0)
            def _():
                for core in range(CORES):
                    ret_copy(chip, core).start()

        for step in range(far - 1, 0, -1):
            r = t - 1 - step

            @pl.when((r >= 0) & (r < n_y))
            def _():
                relay(chip_at(r), step)

        b = t - 1

        @pl.when(b == 0)
        def _():
            sib_arrival().wait_recv()
            load_wg.wait()
            load_wu.wait()

        @pl.when((b >= 0) & (b < n_y))
        def _():
            chip = chip_at(b)

            @pl.when(b > 0)
            def _():
                for side in range(2):
                    x_arrival(chip, side).wait_recv()

            first_layers(chip)

        @pl.when((t > 0) & (t < n_y))
        def _():
            forward(chip_at(t))

        @pl.when(t == 3)
        def _():
            @pl.loop(1, n_tp)
            def _(s):
                x = x_at(s)
                w_arrival(x).wait_recv()
                z_copy(x, wpart).start()

    s_iota = lax.broadcasted_iota(jnp.int32, (tokens, n_ep * CAP), 1).astype(F32)
    pair = jnp.where(s_iota == slot0, gates_ref[:, 0:1], 0.0) + jnp.where(
        s_iota == slot1, gates_ref[:, 1:2], 0.0)
    high = pair.astype(BF)
    low = (pair - high.astype(F32)).astype(BF)

    @pl.loop(1, n_ep)
    def _(s):
        ret_arrival(lax.rem(me_e + s, n_ep)).wait_recv()

    back = ret[...]
    combined = dot(high, back) + dot(low, back)

    sum1 = jnp.sum(combined, axis=1, keepdims=True)
    sum2 = jnp.sum(combined * combined, axis=1, keepdims=True)
    stat[me_x] = jnp.where(lane == 0, sum1, jnp.where(lane == 1, sum2, 0.0)).T[:8]

    def stat_copy(x):
        here = stat.at[me_x]
        return pltpu.make_async_remote_copy(
            here, here, ss_sem.at[x], sr_sem.at[me_x], device_id={"tp": x})

    def stat_arrival(x):
        here = stat.at[x]
        return pltpu.make_async_remote_copy(
            here, here, ss_sem.at[x], sr_sem.at[x], device_id={"tp": x})

    @pl.loop(1, n_tp)
    def _(s):
        stat_copy(x_at(s)).start()

    @pl.loop(1, n_tp)
    def _(s):
        stat_arrival(x_at(s)).wait_recv()

    total = stat[0]
    for j in range(1, n_tp):
        total += stat[j]
    moments = jnp.concatenate([total, jnp.zeros((120, tokens), F32)], axis=0).T
    mean = moments[:, 0:1] / width
    var = moments[:, 1:2] / width - mean * mean
    out_ref[...] = (
        (combined - mean) * lax.rsqrt(var + EPS) * gain_ref[...] + bias_ref[...]
    ).astype(BF)

    @pl.loop(1, n_tp)
    def _(s):
        x = x_at(s)
        w_copy(s - 1).wait_send()
        z_copy(x, wpart).wait_send()
        stat_copy(x).wait_send()

    sib_copy().wait_send()
    ret_copy(me_y, 1 - me_c).wait_send()
    for side in range(2):
        for step in range(1, far + 1):
            hid_copy(me_y, step, side).wait_send()

    @pl.loop(1, n_y)
    def _(i):
        chip = chip_at(i)
        for core in range(CORES):
            y_copy(chip, core).wait_send()
            ret_copy(chip, core).wait_send()
        for side in range(2):
            x_copy(chip, side).wait_send()
            for step in range(1, far + 1):
                hid_copy(chip, step, side).wait_send()


def on_device(sizes, tokens, expert_ids, gates, w_gate, w_up, w_down, norm_gain, norm_bias):
    n_ep, n_tp, n_grp = sizes
    n_y = n_ep // CORES
    tok_rows, width = tokens.shape
    ff = w_gate.shape[2]
    cols = norm_gain.shape[0]
    slots = n_ep * CAP
    far = n_tp // 2
    vmem = pl.BlockSpec(memory_space=pltpu.VMEM)
    hbm = pl.BlockSpec(memory_space=pl.ANY)
    dma = pltpu.SemaphoreType.DMA
    return pl.pallas_call(
        functools.partial(kernel, n_ep, n_tp, n_grp),
        out_shape=jax.ShapeDtypeStruct((tok_rows, cols), BF),
        in_specs=[hbm, vmem, vmem, hbm, hbm, hbm, vmem, vmem],
        out_specs=vmem,
        scratch_shapes=[
            pltpu.VMEM((tok_rows, width), BF),
            pltpu.VMEM((width, ff), BF),
            pltpu.VMEM((width, ff), BF),
            pltpu.VMEM((n_tp * ff, cols), BF),
            pltpu.VMEM((4, slots, width // 4), BF),
            pltpu.VMEM((2, slots, width // 4), BF),
            pltpu.VMEM((4, CAP, width // 4), BF),
            pltpu.VMEM((n_tp, slots, ff), BF),
            pltpu.VMEM((slots, cols), BF),
            pltpu.VMEM((slots, cols), BF),
            pltpu.VMEM((8, tok_rows), F32),
            pltpu.VMEM((n_tp, 8, tok_rows), F32),
            dma((4,)),
            dma((n_ep,)), dma((n_ep,)),
            dma((2, n_y)), dma((2, n_y)),
            dma((2, far, n_y)), dma((2, far, n_y)),
            dma((n_ep,)), dma((n_ep,)),
            dma((n_tp,)), dma((n_tp,)),
            dma((n_tp,)), dma((n_tp,)),
            dma((n_tp,)), dma((n_tp,)),
        ],
        compiler_params=pltpu.CompilerParams(
            collective_id=0, has_side_effects=True, vmem_limit_bytes=60 * 2**20),
    )(
        tokens, expert_ids, gates,
        w_gate.reshape(width, ff), w_up.reshape(width, ff), w_down.reshape(ff, width),
        norm_gain.reshape(1, cols), norm_bias.reshape(1, cols),
    )


def solution(mesh):
    sizes = (mesh.shape["ep"], mesh.shape["tp"], mesh.shape["grp"])
    return jax.shard_map(
        functools.partial(on_device, sizes),
        mesh=mesh,
        in_specs=(
            P(("grp", "ep"), None),
            P(("grp", "ep"), None),
            P(("grp", "ep"), None),
            P("ep", None, "tp"),
            P("ep", None, "tp"),
            P("ep", "tp", None),
            P("tp"),
            P("tp"),
        ),
        out_specs=P(("grp", "ep"), "tp"),
        check_vma=False,
    )
```

time: 359 us -> 170 us (0.47)
  waiting for transfers between devices: 216 us -> 0 us
  Pallas kernels: 0 us -> 165 us
  blocking collectives: 62.7 us -> 0 us
  local copies, waits for them, and re-layouts: 29.6 us -> 4.62 us
  matrix products: 14.4 us -> 0 us
  other arithmetic: 14.4 us -> 0 us
  between operations: 13.7 us -> 0.01 us
  starting transfers between devices: 7.98 us -> 0 us
    pallas_call x0 -> x1, Pallas kernels: none -> 165 us  [on_device(): pl.pallas_call(functools.partial(kernel, n_ep, n_tp, n_grp), out_shape=ja...]
    reduce_scatter x1 -> x0, waiting for transfers between devices: 95.3 us -> none  [on_device(): lax.psum_scatter(partial_value.astype(jnp.bfloat16), 'tp', scatter_dimens...]
    all_gather x1 -> x0, waiting for transfers between devices: 92.8 us -> none  [on_device(): segment = lax.all_gather(arrived, 'tp', axis=2, tiled=True)]
    all_to_all x2 -> x0, blocking collectives: 62.7 us -> none  [the longest x1 52 us: on_device(): lax.all_to_all(outgoing, 'ep', split_axis=0, concat_axis=1, tiled=True)]
    all_to_all x1 -> x0, waiting for transfers between devices: 27.7 us -> none  [on_device(): lax.all_to_all(summed, 'ep', split_axis=1, concat_axis=0, tiled=True)]
    dot_general x3 -> x0, matrix products: 14.4 us -> none  [the longest x1 6.46 us: on_device(): jnp.einsum('erd,edf->erf', segment, w_gate, preferred_element_type=jnp.fl...]
    unnamed x1 -> x0, other arithmetic: 8.25 us -> none
    all_to_all x1 -> x0, starting transfers between devices: 7.73 us -> none  [on_device(): lax.all_to_all(summed, 'ep', split_axis=1, concat_axis=0, tiled=True)]
  transfers between devices with their start and end apart: 3 -> 0, of which waited for: 3 -> 0; matrix products, arithmetic and copies ran while one was open for 0% -> 0% of each run, Pallas kernels for 0% -> 0%
where the time goes in v1:
time: 170 us; the launch traced here: 169 us
  Pallas kernels  165 us (97%)
  local copies, waits for them, and re-layouts  4.62 us (3%)
    pallas_call x1, Pallas kernels, on_device(): pl.pallas_call(functools.partial(kernel, n_ep, n_tp, n_grp), out_shape=ja...  165 us
    unnamed x3, local copies, waits for them, and re-layouts  4.62 us

profile of v1, /device:TPU:513, one launch (start us, length us, event | category | flops | bytes accessed | tf_op | source)
XLA Modules:
  0.0 169.4 jit_solution(4556116506543691327)
XLA Ops:
  0.0 1.5 copy.9.ids_ref
  1.5 1.5 copy.10.gates_ref
  3.0 164.8 %shard_map.82 = bf16[256,512]{1,0:T(8,128)(2,1)} custom-call(bf16[256,4096]{1,0:T(8,128)(2,1)} %tok_hbm.1, s32[256,2]{1,0:T(8,128)} %copy.9.ids_ref, f32[256,2]{1,0:T(8,128)} %copy.10.gates_ref, bf16[4096,256]{1,0:T(8,128)(2,1)} %bitcast.5, bf16[4096,256]{1,0:T(8,128)(2,1)} %bitcast.6, bf16[256,4096]{1,0:T(8,128)(2,1)} %bitcast.7, f32[1,512]{1,0:T(1,128)} %bitcast.8, ...), custom_call_target="tpu_custom_call" | custom-call | tf_op jit(solution)/shard_map/pallas_call | solution.py:401
  167.7 1.7 copy.12

commit v2 on v1

--- a/solution.py
+++ b/solution.py
@@ -18,16 +18,36 @@
     return jnp.dot(a, b, preferred_element_type=F32)
 
 
+FAR = 4
+QUARTER_TYPE, THREE_TYPE, FULL_TYPE = 3, 5, 7
+PLAN = (
+    ("B", 0), ("A", 1), ("W", 0), ("C1", 0), ("A2", 1), ("W", 1),
+    ("A", 2), ("A", 3), ("C2", 0), ("B", 1), ("A2", 2), ("A2", 3),
+    ("C3", 0), ("C1", 1), ("B", 2), ("B", 3), ("D", 0), ("C2", 1),
+    ("C1", 2), ("C1", 3), ("C3", 1), ("C2", 2), ("C2", 3), ("A", 4),
+    ("A", 5), ("D", 1), ("C3", 2), ("C3", 3), ("B", 4), ("B", 5),
+    ("D", 2), ("C1", 4), ("D", 3), ("C1", 5), ("C2", 4), ("C2", 5),
+    ("C3", 4), ("C3", 5), ("D", 4), ("B", 6), ("B", 7), ("D", 5),
+    ("C1", 6), ("C1", 7), ("C2", 6), ("C2", 7), ("C3", 6), ("C3", 7),
+    ("D", 6), ("D", 7),
+)
+STAGES = ("A", "A2", "B", "C1", "C2", "C3", "D", "W")
+
+
 def offset_of(i):
-    half = (i + 1) // 2
-    return half * (2 * lax.rem(i, 2) - 1)
+    size = FAR - i // 2
+    return jnp.where(i == 0, 0, size * (2 * lax.rem(i, 2) - 1))
+
+
+def near_offset(i):
+    return (i // 2 + 1) * (1 - 2 * lax.rem(i, 2))
 
 
 def kernel(
     n_ep, n_tp, n_grp,
     tok_hbm, ids_ref, gates_ref, wg_hbm, wu_hbm, wd_hbm, gain_ref, bias_ref,
     out_ref,
-    tok, wg, wu, wdc, routed, sendb, sib, hid, outb, ret, slots, stat,
+    tok, wg, wu, wdc, routed, sendb, sib, hid, outb, ret, slots, stat, high, low,
     load_sem,
     ys_sem, yr_sem, xs_sem, xr_sem, hs_sem, hr_sem, rs_sem, rr_sem,
     ws_sem, wr_sem, zs_sem, zr_sem, ss_sem, sr_sem,
@@ -41,7 +61,8 @@
     far = n_tp // 2
     me_g, me_e, me_x = (lax.axis_index(a) for a in ("grp", "ep", "tp"))
     me_y, me_c = me_e // CORES, lax.rem(me_e, CORES)
-    half = lax.rem(me_x, 2)
+    kind = lax.rem(me_x, 4)
+    side_cols = (slice(0, quarter // 2), slice(quarter // 2, quarter))
     right, left = lax.rem(me_x + 1, n_tp), lax.rem(me_x + n_tp - 1, n_tp)
     mate = me_g + 1 - 2 * lax.rem(me_g, 2)
     wpart = lax.rem(me_g, 2)
@@ -76,10 +97,12 @@
         pl.semaphore_signal(barrier, 1, device_id={"tp": lax.rem(me_x + s, n_tp)})
     pl.semaphore_signal(barrier, 1, device_id={"grp": mate})
 
-    ids = ids_ref[...]
     lane = lax.broadcasted_iota(jnp.int32, (tokens, 128), 1)
-    hit0 = lane == ids[:, 0:1]
-    hit1 = lane == ids[:, 1:2]
+    columns = jnp.concatenate(
+        [ids_ref[...].astype(F32), gates_ref[...], jnp.zeros((124, tokens), F32)], axis=0).T
+    lane_f = lane.astype(F32)
+    hit0 = lane_f == columns[:, 0:1]
+    hit1 = lane_f == columns[:, 1:2]
     named = jnp.where(hit0 | hit1, 1.0, 0.0).astype(BF)
     t_row = lax.broadcasted_iota(jnp.int32, (tokens, tokens), 0)
     t_col = lax.broadcasted_iota(jnp.int32, (tokens, tokens), 1)
@@ -98,7 +121,7 @@
         return pl.ds(pl.multiple_of(x * ff + part * wrows, wrows), wrows)
 
     def w_copy(i):
-        x = x_at(offset_of(i + 1))
+        x = x_at(near_offset(i))
         return pltpu.make_async_remote_copy(
             wd_hbm.at[
                 pl.ds(pl.multiple_of(wpart * wrows, wrows), wrows),
@@ -131,39 +154,51 @@
         pick = jnp.where(chosen, 1.0, 0.0).astype(BF)
         return dot(pick, tok[:, pl.ds(pl.multiple_of(column, quarter), quarter)]).astype(BF)
 
-    def y_copy(chip, core):
+    def quarter_of(k):
+        return lax.rem(kind + k, 4)
+
+    def y_copy(chip, core, q):
         expert = chip * CORES + core
         return pltpu.make_async_remote_copy(
-            sendb.at[:, block_rows(expert)],
-            routed.at[pl.ds(2 * half, 2), block_rows(me_e)],
-            ys_sem.at[expert], yr_sem.at[me_e], device_id={"ep": expert},
+            sendb.at[q, block_rows(expert)],
+            routed.at[q, block_rows(me_e)],
+            ys_sem.at[q, expert], yr_sem.at[q, me_e], device_id={"ep": expert},
         )
 
-    def y_arrival(block):
-        here = routed.at[pl.ds(2 * half, 2), block_rows(block)]
-        return pltpu.make_async_remote_copy(
-            here, here, ys_sem.at[block], yr_sem.at[block], device_id={"ep": block})
+    def y_arrival(block, q):
+        here = routed.at[q, block_rows(block)]
+        return pltpu.make_async_remote_copy(
+            here, here, ys_sem.at[q, block], yr_sem.at[q, block], device_id={"ep": block})
+
+    def sent_quarters(i):
+        first = jnp.where((i > QUARTER_TYPE) & (i <= THREE_TYPE), 1, 0)
+        return first, jnp.where(i <= QUARTER_TYPE, 1, 4)
 
     sibling = me_y * CORES + 1 - me_c
 
     def sib_copy():
         return pltpu.make_async_remote_copy(
             sib, routed.at[:, block_rows(me_e)],
-            ys_sem.at[sibling], yr_sem.at[me_e], device_id={"ep": sibling},
+            ys_sem.at[0, sibling], yr_sem.at[0, me_e], device_id={"ep": sibling},
         )
 
     def sib_arrival():
         here = routed.at[:, block_rows(sibling)]
         return pltpu.make_async_remote_copy(
-            here, here, ys_sem.at[sibling], yr_sem.at[sibling], device_id={"ep": sibling})
+            here, here, ys_sem.at[0, sibling], yr_sem.at[0, sibling], device_id={"ep": sibling})
 
     @pl.loop(1, n_y)
     def _(i):
         chip = chip_at(i)
-        for q in range(2):
-            sendb[q, chunk_rows(chip), :] = spread(chip, (2 * half + q) * quarter)
-        for core in range(CORES):
-            y_copy(chip, core).start()
+
+        def send(k, carry):
+            q = quarter_of(k)
+            sendb[q, chunk_rows(chip), :] = spread(chip, q * quarter)
+            for core in range(CORES):
+                y_copy(chip, core, q).start()
+            return carry
+
+        lax.fori_loop(*sent_quarters(i), send, 0)
 
     @pl.loop(0, 4)
     def _(q):
@@ -174,17 +209,41 @@
 
     sib_copy().start()
 
-    def x_copy(chip, side):
-        here = routed.at[2 * half + side, chunk_rows(chip)]
-        return pltpu.make_async_remote_copy(
-            here, here, xs_sem.at[side, chip], xr_sem.at[side, chip],
-            device_id={"tp": (right, left)[side]})
-
-    def x_arrival(chip, side):
-        here = routed.at[2 * (1 - half) + side, chunk_rows(chip)]
-        return pltpu.make_async_remote_copy(
-            here, here, xs_sem.at[side, chip], xr_sem.at[side, chip],
-            device_id={"tp": (left, right)[side]})
+    s_iota = lax.broadcasted_iota(jnp.int32, (tokens, n_ep * CAP), 1).astype(F32)
+    pair = jnp.where(s_iota == slot0, columns[:, 2:3], 0.0) + jnp.where(
+        s_iota == slot1, columns[:, 3:4], 0.0)
+    high[...] = pair.astype(BF)
+    low[...] = (pair - high[...].astype(F32)).astype(BF)
+
+    def x_move(part, side, step, chip, arriving):
+        peer = ((right, left), (left, right))[arriving][side]
+        return pltpu.make_async_remote_copy(
+            part, part, xs_sem.at[side, step, chip], xr_sem.at[side, step, chip],
+            device_id={"tp": peer})
+
+    def whole(k, chip):
+        return routed.at[quarter_of(k), chunk_rows(chip)]
+
+    def half_of(k, chip, side):
+        return routed.at[quarter_of(k), chunk_rows(chip), side_cols[side]]
+
+    def x_copy_q(chip, side):
+        return x_move(whole(0, chip), side, 0, chip, False)
+
+    def x_arrival_q(chip, side):
+        return x_move(whole((3, 1)[side], chip), side, 0, chip, True)
+
+    def x_copy_q2(chip, side):
+        return x_move(half_of((3, 1)[side], chip, side), side, 1, chip, False)
+
+    def x_arrival_q2(chip, side):
+        return x_move(half_of(2, chip, side), side, 1, chip, True)
+
+    def x_copy_t(chip, side):
+        return x_move(half_of((1, 3)[side], chip, side), side, 0, chip, False)
+
+    def x_arrival_t(chip, side):
+        return x_move(half_of(0, chip, side), side, 0, chip, True)
 
     def hid_part(chip, x, step, side):
         if step < far:
@@ -217,11 +276,13 @@
         return pltpu.make_async_remote_copy(
             here, here, rs_sem.at[expert], rr_sem.at[expert], device_id={"ep": expert})
 
-    def forward(chip):
-        for core in range(CORES):
-            y_arrival(chip * CORES + core).wait_recv()
-        for side in range(2):
-            x_copy(chip, side).start()
+    def y_wait(i, chip):
+        def one(k, carry):
+            for core in range(CORES):
+                y_arrival(chip * CORES + core, quarter_of(k)).wait_recv()
+            return carry
+
+        lax.fori_loop(*sent_quarters(i), one, 0)
 
     def first_layers(chip):
         here = chunk_rows(chip)
@@ -250,85 +311,106 @@
             acc += dot(hid[j, here, :], wdc[j * ff:(j + 1) * ff, :])
         outb[here, :] = acc.astype(BF)
 
-    stages = far + 2
-    lag_last = stages - 1
-
-    @pl.loop(0, n_y + lag_last)
-    def _(t):
-        c = t - lag_last
-
-        @pl.when(c == 0)
-        def _():
-            @pl.loop(1, n_tp)
-            def _(s):
-                z_copy(x_at(s), 1 - wpart).wait_recv()
-            load_wd.wait()
-
-        @pl.when((c >= 0) & (c < n_y))
-        def _():
-            chip = chip_at(c)
+    def at_event(e):
+        code = jnp.int32(0)
+        for n, (stage, i) in enumerate(PLAN):
+            code = jnp.where(e == n, STAGES.index(stage) * n_y + i, code)
+        return code // n_y, lax.rem(code, n_y)
+
+    @pl.loop(0, len(PLAN))
+    def _(e):
+        stage, i = at_event(e)
+        chip = chip_at(i)
+
+        def when(name):
+            return pl.when(stage == STAGES.index(name))
+
+        @when("A")
+        def _():
+            y_wait(i, chip)
+
+            @pl.when(i <= QUARTER_TYPE)
+            def _():
+                for side in range(2):
+                    x_copy_q(chip, side).start()
+
+            @pl.when(i > QUARTER_TYPE)
+            def _():
+                for side in range(2):
+                    x_copy_t(chip, side).start()
+
+        @when("A2")
+        def _():
+            for side in range(2):
+                x_arrival_q(chip, side).wait_recv()
+                x_copy_q2(chip, side).start()
+
+        @when("B")
+        def _():
+            @pl.when(i == 0)
+            def _():
+                sib_arrival().wait_recv()
+                load_wg.wait()
+                load_wu.wait()
+
+            @pl.when((i > 0) & (i <= QUARTER_TYPE))
+            def _():
+                for side in range(2):
+                    x_arrival_q2(chip, side).wait_recv()
+
+            @pl.when((i > QUARTER_TYPE) & (i <= THREE_TYPE))
+            def _():
+                for side in range(2):
+                    x_arrival_t(chip, side).wait_recv()
+
+            @pl.when(i > THREE_TYPE)
+            def _():
+                y_wait(i, chip)
+
+            first_layers(chip)
+
+        for step in range(1, far):
+            @when(f"C{step}")
+            def _():
+                relay(chip, step)
+
+        @when("W")
+        def _():
+            for n in range(n_tp // 2):
+                @pl.when((i == 0) == (n < n_tp // 4))
+                def _():
+                    for s in sorted({n + 1, -n - 1 + n_tp}):
+                        x = x_at(s)
+                        w_arrival(x).wait_recv()
+                        z_copy(x, wpart).start()
+
+        @when("D")
+        def _():
+            @pl.when(i == 0)
+            def _():
+                @pl.loop(1, n_tp)
+                def _(s):
+                    z_copy(x_at(s), 1 - wpart).wait_recv()
+                load_wd.wait()
+
             last_layer(chip)
 
-            @pl.when(c == 0)
+            @pl.when(i == 0)
             def _():
                 ret[block_rows(me_e), :] = outb[block_rows(me_e), :]
                 ret_copy(me_y, 1 - me_c).start()
 
-            @pl.when(c > 0)
+            @pl.when(i > 0)
             def _():
                 for core in range(CORES):
                     ret_copy(chip, core).start()
-
-        for step in range(far - 1, 0, -1):
-            r = t - 1 - step
-
-            @pl.when((r >= 0) & (r < n_y))
-            def _():
-                relay(chip_at(r), step)
-
-        b = t - 1
-
-        @pl.when(b == 0)
-        def _():
-            sib_arrival().wait_recv()
-            load_wg.wait()
-            load_wu.wait()
-
-        @pl.when((b >= 0) & (b < n_y))
-        def _():
-            chip = chip_at(b)
-
-            @pl.when(b > 0)
-            def _():
-                for side in range(2):
-                    x_arrival(chip, side).wait_recv()
-
-            first_layers(chip)
-
-        @pl.when((t > 0) & (t < n_y))
-        def _():
-            forward(chip_at(t))
-
-        @pl.when(t == 3)
-        def _():
-            @pl.loop(1, n_tp)
-            def _(s):
-                x = x_at(s)
-                w_arrival(x).wait_recv()
-                z_copy(x, wpart).start()
-
-    s_iota = lax.broadcasted_iota(jnp.int32, (tokens, n_ep * CAP), 1).astype(F32)
-    pair = jnp.where(s_iota == slot0, gates_ref[:, 0:1], 0.0) + jnp.where(
-        s_iota == slot1, gates_ref[:, 1:2], 0.0)
-    high = pair.astype(BF)
-    low = (pair - high.astype(F32)).astype(BF)
 
     @pl.loop(1, n_ep)
     def _(s):
         ret_arrival(lax.rem(me_e + s, n_ep)).wait_recv()
 
     back = ret[...]
-    combined = dot(high, back) + dot(low, back)
+    combined = dot(high[...], back) + dot(low[...], back)
 
     sum1 = jnp.sum(combined, axis=1, keepdims=True)
     sum2 = jnp.sum(combined * combined, axis=1, keepdims=True)
@@ -378,11 +460,28 @@
     @pl.loop(1, n_y)
     def _(i):
         chip = chip_at(i)
+
+        def gone(k, carry):
+            for core in range(CORES):
+                y_copy(chip, core, quarter_of(k)).wait_send()
+            return carry
+
+        lax.fori_loop(*sent_quarters(i), gone, 0)
         for core in range(CORES):
-            y_copy(chip, core).wait_send()
             ret_copy(chip, core).wait_send()
+
+        @pl.when(i <= QUARTER_TYPE)
+        def _():
+            for side in range(2):
+                x_copy_q(chip, side).wait_send()
+                x_copy_q2(chip, side).wait_send()
+
+        @pl.when((i > QUARTER_TYPE) & (i <= THREE_TYPE))
+        def _():
+            for side in range(2):
+                x_copy_t(chip, side).wait_send()
+
         for side in range(2):
-            x_copy(chip, side).wait_send()
             for step in range(1, far + 1):
                 hid_copy(chip, step, side).wait_send()
 
@@ -409,16 +508,18 @@
             pltpu.VMEM((width, ff), BF),
             pltpu.VMEM((n_tp * ff, cols), BF),
             pltpu.VMEM((4, slots, width // 4), BF),
-            pltpu.VMEM((2, slots, width // 4), BF),
+            pltpu.VMEM((4, slots, width // 4), BF),
             pltpu.VMEM((4, CAP, width // 4), BF),
             pltpu.VMEM((n_tp, slots, ff), BF),
             pltpu.VMEM((slots, cols), BF),
             pltpu.VMEM((slots, cols), BF),
             pltpu.VMEM((8, tok_rows), F32),
             pltpu.VMEM((n_tp, 8, tok_rows), F32),
+            pltpu.VMEM((tok_rows, slots), BF),
+            pltpu.VMEM((tok_rows, slots), BF),
             dma((4,)),
-            dma((n_ep,)), dma((n_ep,)),
-            dma((2, n_y)), dma((2, n_y)),
+            dma((4, n_ep)), dma((4, n_ep)),
+            dma((2, 2, n_y)), dma((2, 2, n_y)),
             dma((2, far, n_y)), dma((2, far, n_y)),
             dma((n_ep,)), dma((n_ep,)),
             dma((n_tp,)), dma((n_tp,)),
@@ -428,7 +529,7 @@
         compiler_params=pltpu.CompilerParams(
             collective_id=0, has_side_effects=True, vmem_limit_bytes=60 * 2**20),
     )(
-        tokens, expert_ids, gates,
+        tokens, expert_ids.T, gates.T,
         w_gate.reshape(width, ff), w_up.reshape(width, ff), w_down.reshape(ff, width),
         norm_gain.reshape(1, cols), norm_bias.reshape(1, cols),
     )

time: 170 us -> 151 us (0.89)
  Pallas kernels: 165 us -> 149 us
  local copies, waits for them, and re-layouts: 4.62 us -> 1.67 us
    pallas_call x1, Pallas kernels: 165 us -> 149 us  [on_device(): pl.pallas_call(functools.partial(kernel, n_ep, n_tp, n_grp), out_shape=ja...]
    unnamed x3 -> x1, local copies, waits for them, and re-layouts: 4.62 us -> 1.67 us
where the time goes in v2:
time: 151 us
  Pallas kernels  149 us (99%)
  local copies, waits for them, and re-layouts  1.67 us (1%)
    pallas_call x1, Pallas kernels, on_device(): pl.pallas_call(functools.partial(kernel, n_ep, n_tp, n_grp), out_shape=ja...  149 us

profile of v2, /device:TPU:513, one launch (start us, length us, event | category | flops | bytes accessed | tf_op | source)
XLA Modules:
  0.0 150.6 jit_solution(6734043275996070474)
XLA Ops:
  0.0 148.9 %shard_map.82 = bf16[256,512]{1,0:T(8,128)(2,1)} custom-call(bf16[256,4096]{1,0:T(8,128)(2,1)} %tok_hbm.1, s32[2,256]{1,0:T(2,128)} %bitcast.10, f32[2,256]{1,0:T(2,128)} %bitcast.11, bf16[4096,256]{1,0:T(8,128)(2,1)} %bitcast.7, bf16[4096,256]{1,0:T(8,128)(2,1)} %bitcast.8, bf16[256,4096]{1,0:T(8,128)(2,1)} %bitcast.9, f32[1,512]{1,0:T(1,128)} %bitcast.12, ...), custom_call_target="tpu_custom_call" | custom-call | tf_op jit(solution)/shard_map/pallas_call | solution.py:500
  148.9 1.7 %copy.10 = bf16[256,512]{1,0:T(8,128)(2,1)} copy(bf16[256,512]{1,0:T(8,128)(2,1)} %shard_map.82) | data formatting | bytes 524288

commit v3 on v2

--- a/solution.py
+++ b/solution.py
@@ -18,25 +18,35 @@
     return jnp.dot(a, b, preferred_element_type=F32)
 
 
-FAR = 4
-QUARTER_TYPE, THREE_TYPE, FULL_TYPE = 3, 5, 7
+OFFSETS = (0, 3, -3, 4, 2, -2, 1, -1)
+QUARTERS = {0: (0, 4, 1), 1: (0, 4, 1), 2: (0, 2, 2), 3: (0, 1, 1), 4: (0, 1, 1)}
+STAGES = ("S", "W", "O", "G", "Y", "A", "A2", "B", "C1", "C2", "C3", "D")
 PLAN = (
-    ("B", 0), ("A", 1), ("W", 0), ("C1", 0), ("A2", 1), ("W", 1),
-    ("A", 2), ("A", 3), ("C2", 0), ("B", 1), ("A2", 2), ("A2", 3),
-    ("C3", 0), ("C1", 1), ("B", 2), ("B", 3), ("D", 0), ("C2", 1),
-    ("C1", 2), ("C1", 3), ("C3", 1), ("C2", 2), ("C2", 3), ("A", 4),
-    ("A", 5), ("D", 1), ("C3", 2), ("C3", 3), ("B", 4), ("B", 5),
-    ("D", 2), ("C1", 4), ("D", 3), ("C1", 5), ("C2", 4), ("C2", 5),
-    ("C3", 4), ("C3", 5), ("D", 4), ("B", 6), ("B", 7), ("D", 5),
-    ("C1", 6), ("C1", 7), ("C2", 6), ("C2", 7), ("C3", 6), ("C3", 7),
-    ("D", 6), ("D", 7),
+    ("S", 2), ("S", 3), ("S", 1), ("Y", 2), ("Y", 1), ("S", 0),
+    ("Y", 3), ("G", 0), ("A", 2), ("Y", 5), ("O", 0), ("Y", 7),
+    ("W", 0), ("Y", 4), ("A", 1), ("A2", 2), ("W", 1), ("A", 3),
+    ("A2", 1), ("A2", 3), ("B", 2), ("B", 0), ("B", 1), ("Y", 6),
+    ("C1", 2), ("B", 3), ("A", 4), ("C1", 1), ("A", 5), ("C1", 3),
+    ("C2", 1), ("C2", 2), ("B", 4), ("B", 5), ("C2", 3), ("C3", 1),
+    ("C3", 2), ("B", 6), ("C3", 3), ("C1", 4), ("C1", 5), ("B", 7),
+    ("D", 1), ("D", 2), ("C1", 0), ("C2", 5), ("C2", 4), ("C1", 6),
+    ("C1", 7), ("D", 3), ("C3", 4), ("C3", 5), ("C2", 6), ("C2", 7),
+    ("D", 4), ("C2", 0), ("D", 5), ("C3", 6), ("C3", 7), ("D", 6),
+    ("C3", 0), ("D", 7), ("D", 0),
 )
-STAGES = ("A", "A2", "B", "C1", "C2", "C3", "D", "W")
+FIRST_B, FIRST_D = 2, 1
+RETURNS = (2, 1, 3, 5, 4, 7, 6, 0)
+
+
+def among(i, values):
+    out = jnp.int32(values[0])
+    for n, value in enumerate(values[1:], 1):
+        out = jnp.where(i == n, value, out)
+    return out
 
 
 def offset_of(i):
-    size = FAR - i // 2
-    return jnp.where(i == 0, 0, size * (2 * lax.rem(i, 2) - 1))
+    return among(i, OFFSETS)
 
 
 def near_offset(i):
@@ -47,7 +57,7 @@
     n_ep, n_tp, n_grp,
     tok_hbm, ids_ref, gates_ref, wg_hbm, wu_hbm, wd_hbm, gain_ref, bias_ref,
     out_ref,
-    tok, wg, wu, wdc, routed, sendb, sib, hid, outb, ret, slots, stat, high, low,
+    tok, wg, wu, wdc, routed, sendb, sib, hid, outb, ret, slots, stat, high, low, mixed,
     load_sem,
     ys_sem, yr_sem, xs_sem, xr_sem, hs_sem, hr_sem, rs_sem, rr_sem,
     ws_sem, wr_sem, zs_sem, zr_sem, ss_sem, sr_sem,
@@ -85,17 +95,17 @@
     own_cols = pl.ds(pl.multiple_of(me_x * cols, cols), cols)
     own_w = pl.ds(pl.multiple_of(me_x * ff, ff), ff)
     load_wd = pltpu.make_async_copy(wd_hbm.at[:, own_cols], wdc.at[own_w], load_sem.at[3])
-    load_tok.start()
-    load_wg.start()
-    load_wu.start()
-    load_wd.start()
-
     barrier = pltpu.get_barrier_semaphore()
     for s in range(1, n_ep):
         pl.semaphore_signal(barrier, 1, device_id={"ep": lax.rem(me_e + s, n_ep)})
     for s in range(1, n_tp):
         pl.semaphore_signal(barrier, 1, device_id={"tp": lax.rem(me_x + s, n_tp)})
     pl.semaphore_signal(barrier, 1, device_id={"grp": mate})
+
+    load_tok.start()
+    load_wg.start()
+    load_wu.start()
+    load_wd.start()
 
     lane = lax.broadcasted_iota(jnp.int32, (tokens, 128), 1)
     columns = jnp.concatenate(
@@ -141,11 +151,6 @@
         return pltpu.make_async_remote_copy(
             here, here, zs_sem.at[x], zr_sem.at[x], device_id={"grp": mate})
 
-    @pl.loop(0, n_tp - 1)
-    def _(i):
-        w_copy(i).start()
-
-    load_tok.wait()
 
     def spread(chip, column):
         s_iota = (chip * rows).astype(F32) + lax.broadcasted_iota(
@@ -170,9 +175,15 @@
         return pltpu.make_async_remote_copy(
             here, here, ys_sem.at[q, block], yr_sem.at[q, block], device_id={"ep": block})
 
-    def sent_quarters(i):
-        first = jnp.where((i > QUARTER_TYPE) & (i <= THREE_TYPE), 1, 0)
-        return first, jnp.where(i <= QUARTER_TYPE, 1, 4)
+    def each_quarter(i, act):
+        spec = [QUARTERS[abs(d)] for d in OFFSETS]
+        first, number, stride = (among(i, [q[n] for q in spec]) for n in range(3))
+
+        def one(k, carry):
+            act(quarter_of(first + k * stride))
+            return carry
+
+        lax.fori_loop(0, number, one, 0)
 
     sibling = me_y * CORES + 1 - me_c
 
@@ -187,33 +198,23 @@
         return pltpu.make_async_remote_copy(
             here, here, ys_sem.at[0, sibling], yr_sem.at[0, sibling], device_id={"ep": sibling})
 
-    @pl.loop(1, n_y)
-    def _(i):
-        chip = chip_at(i)
-
-        def send(k, carry):
-            q = quarter_of(k)
+    def dispatch(i, chip):
+        def send(q):
             sendb[q, chunk_rows(chip), :] = spread(chip, q * quarter)
             for core in range(CORES):
                 y_copy(chip, core, q).start()
-            return carry
-
-        lax.fori_loop(*sent_quarters(i), send, 0)
-
-    @pl.loop(0, 4)
-    def _(q):
-        both = spread(me_y, q * quarter)
-        swap = me_c == 0
-        routed[q, block_rows(me_e), :] = jnp.where(swap, both[:CAP], both[CAP:])
-        sib[q] = jnp.where(swap, both[CAP:], both[:CAP])
-
-    sib_copy().start()
-
-    s_iota = lax.broadcasted_iota(jnp.int32, (tokens, n_ep * CAP), 1).astype(F32)
-    pair = jnp.where(s_iota == slot0, columns[:, 2:3], 0.0) + jnp.where(
-        s_iota == slot1, columns[:, 3:4], 0.0)
-    high[...] = pair.astype(BF)
-    low[...] = (pair - high[...].astype(F32)).astype(BF)
+
+        each_quarter(i, send)
+
+    def own_rows():
+        @pl.loop(0, 4)
+        def _(q):
+            both = spread(me_y, q * quarter)
+            swap = me_c == 0
+            routed[q, block_rows(me_e), :] = jnp.where(swap, both[:CAP], both[CAP:])
+            sib[q] = jnp.where(swap, both[CAP:], both[:CAP])
+
+        sib_copy().start()
 
     def x_move(part, side, step, chip, arriving):
         peer = ((right, left), (left, right))[arriving][side]
@@ -238,12 +239,6 @@
 
     def x_arrival_q2(chip, side):
         return x_move(half_of(2, chip, side), side, 1, chip, True)
-
-    def x_copy_t(chip, side):
-        return x_move(half_of((1, 3)[side], chip, side), side, 0, chip, False)
-
-    def x_arrival_t(chip, side):
-        return x_move(half_of(0, chip, side), side, 0, chip, True)
 
     def hid_part(chip, x, step, side):
         if step < far:
@@ -277,12 +272,11 @@
             here, here, rs_sem.at[expert], rr_sem.at[expert], device_id={"ep": expert})
 
     def y_wait(i, chip):
-        def one(k, carry):
+        def arrived(q):
             for core in range(CORES):
-                y_arrival(chip * CORES + core, quarter_of(k)).wait_recv()
-            return carry
-
-        lax.fori_loop(*sent_quarters(i), one, 0)
+                y_arrival(chip * CORES + core, q).wait_recv()
+
+        each_quarter(i, arrived)
 
     def first_layers(chip):
         here = chunk_rows(chip)
@@ -311,68 +305,34 @@
             acc += dot(hid[j, here, :], wdc[j * ff:(j + 1) * ff, :])
         outb[here, :] = acc.astype(BF)
 
-    def at_event(e):
-        code = jnp.int32(0)
-        for n, (stage, i) in enumerate(PLAN):
-            code = jnp.where(e == n, STAGES.index(stage) * n_y + i, code)
-        return code // n_y, lax.rem(code, n_y)
+    def pair_weights():
+        s_iota = lax.broadcasted_iota(jnp.int32, (tokens, n_ep * CAP), 1).astype(F32)
+        pair = jnp.where(s_iota == slot0, columns[:, 2:3], 0.0) + jnp.where(
+            s_iota == slot1, columns[:, 3:4], 0.0)
+        high[...] = pair.astype(BF)
+        low[...] = (pair - high[...].astype(F32)).astype(BF)
+
+    def is_sent(i, number):
+        return among(i, [QUARTERS[abs(d)][1] for d in OFFSETS]) == number
+
+    load_tok.wait()
 
     @pl.loop(0, len(PLAN))
     def _(e):
-        stage, i = at_event(e)
+        code = among(e, [STAGES.index(stage) * n_y + i for stage, i in PLAN])
+        stage, i = code // n_y, lax.rem(code, n_y)
         chip = chip_at(i)
 
         def when(name):
             return pl.when(stage == STAGES.index(name))
 
-        @when("A")
-        def _():
-            y_wait(i, chip)
-
-            @pl.when(i <= QUARTER_TYPE)
-            def _():
-                for side in range(2):
-                    x_copy_q(chip, side).start()
-
-            @pl.when(i > QUARTER_TYPE)
-            def _():
-                for side in range(2):
-                    x_copy_t(chip, side).start()
-
-        @when("A2")
-        def _():
-            for side in range(2):
-                x_arrival_q(chip, side).wait_recv()
-                x_copy_q2(chip, side).start()
-
-        @when("B")
-        def _():
-            @pl.when(i == 0)
-            def _():
-                sib_arrival().wait_recv()
-                load_wg.wait()
-                load_wu.wait()
-
-            @pl.when((i > 0) & (i <= QUARTER_TYPE))
-            def _():
-                for side in range(2):
-                    x_arrival_q2(chip, side).wait_recv()
-
-            @pl.when((i > QUARTER_TYPE) & (i <= THREE_TYPE))
-            def _():
-                for side in range(2):
-                    x_arrival_t(chip, side).wait_recv()
-
-            @pl.when(i > THREE_TYPE)
-            def _():
-                y_wait(i, chip)
-
-            first_layers(chip)
-
-        for step in range(1, far):
-            @when(f"C{step}")
-            def _():
-                relay(chip, step)
+        @when("S")
+        def _():
+            w_copy(2 * i).start()
+
+            @pl.when(i < n_tp // 2 - 1)
+            def _():
+                w_copy(2 * i + 1).start()
 
         @when("W")
         def _():
@@ -384,9 +344,65 @@
                         w_arrival(x).wait_recv()
                         z_copy(x, wpart).start()
 
+        @when("O")
+        def _():
+            own_rows()
+
+        @when("G")
+        def _():
+            pair_weights()
+
+        @when("Y")
+        def _():
+            dispatch(i, chip)
+
+        @when("A")
+        def _():
+            y_wait(i, chip)
+            for side in range(2):
+                x_copy_q(chip, side).start()
+
+        @when("A2")
+        def _():
+            for side in range(2):
+                x_arrival_q(chip, side).wait_recv()
+                x_copy_q2(chip, side).start()
+
+        @when("B")
+        def _():
+            @pl.when(i == FIRST_B)
+            def _():
+                load_wg.wait()
+                load_wu.wait()
+
+            @pl.when(i == 0)
+            def _():
+                sib_arrival().wait_recv()
+
+            @pl.when((i > 0) & is_sent(i, 1))
+            def _():
+                for side in range(2):
+                    x_arrival_q2(chip, side).wait_recv()
+
+            @pl.when((i > 0) & is_sent(i, 2))
+            def _():
+                for side in range(2):
+                    x_arrival_q(chip, side).wait_recv()
+
+            @pl.when((i > 0) & is_sent(i, 4))
+            def _():
+                y_wait(i, chip)
+
+            first_layers(chip)
+
+        for step in range(1, far):
+            @when(f"C{step}")
+            def _():
+                relay(chip, step)
+
         @when("D")
         def _():
-            @pl.when(i == 0)
+            @pl.when(i == FIRST_D)
             def _():
                 @pl.loop(1, n_tp)
                 def _(s):
@@ -405,12 +421,27 @@
                 for core in range(CORES):
                     ret_copy(chip, core).start()
 
-    @pl.loop(1, n_ep)
-    def _(s):
-        ret_arrival(lax.rem(me_e + s, n_ep)).wait_recv()
-
-    back = ret[...]
-    combined = dot(high[...], back) + dot(low[...], back)
+    mixed[...] = jnp.zeros_like(mixed)
+
+    @pl.loop(0, n_y)
+    def _(n):
+        i = among(n, RETURNS)
+        chip = chip_at(i)
+
+        @pl.when(i == 0)
+        def _():
+            ret_arrival(sibling).wait_recv()
+
+        @pl.when(i > 0)
+        def _():
+            for core in range(CORES):
+                ret_arrival(chip * CORES + core).wait_recv()
+
+        back = ret[chunk_rows(chip), :]
+        at = chunk_rows(chip)
+        mixed[...] += dot(high[:, at], back) + dot(low[:, at], back)
+
+    combined = mixed[...]
 
     sum1 = jnp.sum(combined, axis=1, keepdims=True)
     sum2 = jnp.sum(combined * combined, axis=1, keepdims=True)
@@ -432,7 +463,43 @@
 
     @pl.loop(1, n_tp)
     def _(s):
+        w_copy(s - 1).wait_send()
+        z_copy(x_at(s), wpart).wait_send()
+
+    sib_copy().wait_send()
+    ret_copy(me_y, 1 - me_c).wait_send()
+    for side in range(2):
+        for step in range(1, far + 1):
+            hid_copy(me_y, step, side).wait_send()
+
+    @pl.loop(1, n_y)
+    def _(i):
+        chip = chip_at(i)
+        for core in range(CORES):
+            ret_copy(chip, core).wait_send()
+
+        def gone(q):
+            for core in range(CORES):
+                y_copy(chip, core, q).wait_send()
+
+        each_quarter(i, gone)
+
+        for side in range(2):
+            @pl.when(jnp.logical_not(is_sent(i, 4)))
+            def _():
+                x_copy_q(chip, side).wait_send()
+
+            @pl.when(is_sent(i, 1))
+            def _():
+                x_copy_q2(chip, side).wait_send()
+
+            for step in range(1, far + 1):
+                hid_copy(chip, step, side).wait_send()
+
+    @pl.loop(1, n_tp)
+    def _(s):
         stat_arrival(x_at(s)).wait_recv()
+        stat_copy(x_at(s)).wait_send()
 
     total = stat[0]
     for j in range(1, n_tp):
@@ -443,47 +510,6 @@
     out_ref[...] = (
         (combined - mean) * lax.rsqrt(var + EPS) * gain_ref[...] + bias_ref[...]
     ).astype(BF)
-
-    @pl.loop(1, n_tp)
-    def _(s):
-        x = x_at(s)
-        w_copy(s - 1).wait_send()
-        z_copy(x, wpart).wait_send()
-        stat_copy(x).wait_send()
-
-    sib_copy().wait_send()
-    ret_copy(me_y, 1 - me_c).wait_send()
-    for side in range(2):
-        for step in range(1, far + 1):
-            hid_copy(me_y, step, side).wait_send()
-
-    @pl.loop(1, n_y)
-    def _(i):
-        chip = chip_at(i)
-
-        def gone(k, carry):
-            for core in range(CORES):
-                y_copy(chip, core, quarter_of(k)).wait_send()
-            return carry
-
-        lax.fori_loop(*sent_quarters(i), gone, 0)
-        for core in range(CORES):
-            ret_copy(chip, core).wait_send()
-
-        @pl.when(i <= QUARTER_TYPE)
-        def _():
-            for side in range(2):
-                x_copy_q(chip, side).wait_send()
-                x_copy_q2(chip, side).wait_send()
-
-        @pl.when((i > QUARTER_TYPE) & (i <= THREE_TYPE))
-        def _():
-            for side in range(2):
-                x_copy_t(chip, side).wait_send()
-
-        for side in range(2):
-            for step in range(1, far + 1):
-                hid_copy(chip, step, side).wait_send()
 
 
 def on_device(sizes, tokens, expert_ids, gates, w_gate, w_up, w_down, norm_gain, norm_bias):
@@ -517,6 +543,7 @@
             pltpu.VMEM((n_tp, 8, tok_rows), F32),
             pltpu.VMEM((tok_rows, slots), BF),
             pltpu.VMEM((tok_rows, slots), BF),
+            pltpu.VMEM((tok_rows, cols), F32),
             dma((4,)),
             dma((4, n_ep)), dma((4, n_ep)),
             dma((2, 2, n_y)), dma((2, 2, n_y)),

time: 151 us -> 145 us (0.960)
  Pallas kernels: 149 us -> 143 us
    pallas_call x1, Pallas kernels: 149 us -> 143 us  [on_device(): pl.pallas_call(functools.partial(kernel, n_ep, n_tp, n_grp), out_shape=ja...]
where the time goes in v3:
time: 145 us
  Pallas kernels  143 us (99%)
  local copies, waits for them, and re-layouts  1.67 us (1%)
    pallas_call x1, Pallas kernels, on_device(): pl.pallas_call(functools.partial(kernel, n_ep, n_tp, n_grp), out_shape=ja...  143 us

profile of v3, /device:TPU:513, one launch (start us, length us, event | category | flops | bytes accessed | tf_op | source)
XLA Modules:
  0.0 144.7 jit_solution(15568435660422186620)
XLA Ops:
  0.0 143.0 %shard_map.82 = bf16[256,512]{1,0:T(8,128)(2,1)} custom-call(bf16[256,4096]{1,0:T(8,128)(2,1)} %tok_hbm.1, s32[2,256]{1,0:T(2,128)} %bitcast.10, f32[2,256]{1,0:T(2,128)} %bitcast.11, bf16[4096,256]{1,0:T(8,128)(2,1)} %bitcast.7, bf16[4096,256]{1,0:T(8,128)(2,1)} %bitcast.8, bf16[256,4096]{1,0:T(8,128)(2,1)} %bitcast.9, f32[1,512]{1,0:T(1,128)} %bitcast.12, ...), custom_call_target="tpu_custom_call" | custom-call | tf_op jit(solution)/shard_map/pallas_call | solution.py:526
  143.0 1.7 %copy.10 = bf16[256,512]{1,0:T(8,128)(2,1)} copy(bf16[256,512]{1,0:T(8,128)(2,1)} %shard_map.82) | data formatting | bytes 524288

commit v4 on v3

--- a/solution.py
+++ b/solution.py
@@ -22,20 +22,20 @@
 QUARTERS = {0: (0, 4, 1), 1: (0, 4, 1), 2: (0, 2, 2), 3: (0, 1, 1), 4: (0, 1, 1)}
 STAGES = ("S", "W", "O", "G", "Y", "A", "A2", "B", "C1", "C2", "C3", "D")
 PLAN = (
-    ("S", 2), ("S", 3), ("S", 1), ("Y", 2), ("Y", 1), ("S", 0),
-    ("Y", 3), ("G", 0), ("A", 2), ("Y", 5), ("O", 0), ("Y", 7),
-    ("W", 0), ("Y", 4), ("A", 1), ("A2", 2), ("W", 1), ("A", 3),
-    ("A2", 1), ("A2", 3), ("B", 2), ("B", 0), ("B", 1), ("Y", 6),
-    ("C1", 2), ("B", 3), ("A", 4), ("C1", 1), ("A", 5), ("C1", 3),
-    ("C2", 1), ("C2", 2), ("B", 4), ("B", 5), ("C2", 3), ("C3", 1),
-    ("C3", 2), ("B", 6), ("C3", 3), ("C1", 4), ("C1", 5), ("B", 7),
-    ("D", 1), ("D", 2), ("C1", 0), ("C2", 5), ("C2", 4), ("C1", 6),
-    ("C1", 7), ("D", 3), ("C3", 4), ("C3", 5), ("C2", 6), ("C2", 7),
-    ("D", 4), ("C2", 0), ("D", 5), ("C3", 6), ("C3", 7), ("D", 6),
-    ("C3", 0), ("D", 7), ("D", 0),
+    ("S", 0), ("Y", 2), ("S", 3), ("Y", 1), ("Y", 3), ("Y", 5),
+    ("S", 2), ("Y", 4), ("Y", 6), ("O", 0), ("S", 1), ("Y", 7),
+    ("G", 0), ("A", 2), ("A", 1), ("B", 0), ("A2", 2), ("A2", 1),
+    ("A", 3), ("B", 2), ("W", 1), ("B", 1), ("A2", 3), ("C1", 2),
+    ("C1", 1), ("A", 4), ("A", 5), ("C2", 2), ("B", 3), ("W", 0),
+    ("B", 4), ("B", 5), ("C3", 2), ("C2", 1), ("C1", 3), ("C1", 4),
+    ("C1", 5), ("C3", 1), ("B", 7), ("D", 2), ("C2", 3), ("B", 6),
+    ("C2", 4), ("C2", 5), ("D", 1), ("C3", 3), ("C1", 6), ("C3", 4),
+    ("C1", 7), ("C1", 0), ("C3", 5), ("D", 3), ("C2", 6), ("D", 4),
+    ("C2", 7), ("D", 5), ("C2", 0), ("C3", 6), ("C3", 7), ("C3", 0),
+    ("D", 6), ("D", 7), ("D", 0),
 )
-FIRST_B, FIRST_D = 2, 1
-RETURNS = (2, 1, 3, 5, 4, 7, 6, 0)
+FIRST_B, FIRST_D = 0, 2
+RETURNS = (1, 2, 3, 5, 4, 7, 6, 0)
 
 
 def among(i, values):

time: 145 us -> 144 us (level)
  no operation moved by 1% of the time
where the time goes in v4:
time: 144 us
  Pallas kernels  142 us (99%)
  local copies, waits for them, and re-layouts  1.67 us (1%)
    pallas_call x1, Pallas kernels, on_device(): pl.pallas_call(functools.partial(kernel, n_ep, n_tp, n_grp), out_shape=ja...  142 us

profile of v4, /device:TPU:513, one launch (start us, length us, event | category | flops | bytes accessed | tf_op | source)
XLA Modules:
  0.0 143.8 jit_solution(3388028557575295058)
XLA Ops:
  0.0 142.1 %shard_map.82 = bf16[256,512]{1,0:T(8,128)(2,1)} custom-call(bf16[256,4096]{1,0:T(8,128)(2,1)} %tok_hbm.1, s32[2,256]{1,0:T(2,128)} %bitcast.10, f32[2,256]{1,0:T(2,128)} %bitcast.11, bf16[4096,256]{1,0:T(8,128)(2,1)} %bitcast.7, bf16[4096,256]{1,0:T(8,128)(2,1)} %bitcast.8, bf16[256,4096]{1,0:T(8,128)(2,1)} %bitcast.9, f32[1,512]{1,0:T(1,128)} %bitcast.12, ...), custom_call_target="tpu_custom_call" | custom-call | tf_op jit(solution)/shard_map/pallas_call | solution.py:526
  142.1 1.7 %copy.10 = bf16[256,512]{1,0:T(8,128)(2,1)} copy(bf16[256,512]{1,0:T(8,128)(2,1)} %shard_map.82) | data formatting | bytes 524288

commit v5 on v4

--- a/solution.py
+++ b/solution.py
@@ -297,12 +297,19 @@
             hid_copy(chip, step + 1, side).start()
 
     def last_layer(chip):
+        here = chunk_rows(chip)
+
+        def term(s):
+            x = x_at(s)
+            at = pl.ds(pl.multiple_of(x * ff, ff), ff)
+            return dot(hid[x, here, :], wdc[at, :])
+
+        acc = term(0)
+        for s in range(1, far):
+            acc += term(s) + term(-s)
         for side in range(2):
             hid_arrival(chip, far, side).wait_recv()
-        here = chunk_rows(chip)
-        acc = jnp.zeros((rows, cols), F32)
-        for j in range(n_tp):
-            acc += dot(hid[j, here, :], wdc[j * ff:(j + 1) * ff, :])
+        acc += term(far)
         outb[here, :] = acc.astype(BF)
 
     def pair_weights():

time: 144 us -> 144 us (level)
  no operation moved by 1% of the time
where the time goes in v5:
time: 144 us
  Pallas kernels  142 us (99%)
  local copies, waits for them, and re-layouts  1.67 us (1%)
    pallas_call x1, Pallas kernels, on_device(): pl.pallas_call(functools.partial(kernel, n_ep, n_tp, n_grp), out_shape=ja...  142 us

profile of v5, /device:TPU:513, one launch (start us, length us, event | category | flops | bytes accessed | tf_op | source)
XLA Modules:
  0.0 143.7 jit_solution(14345727656248625643)
XLA Ops:
  0.0 142.1 %shard_map.82 = bf16[256,512]{1,0:T(8,128)(2,1)} custom-call(bf16[256,4096]{1,0:T(8,128)(2,1)} %tok_hbm.1, s32[2,256]{1,0:T(2,128)} %bitcast.10, f32[2,256]{1,0:T(2,128)} %bitcast.11, bf16[4096,256]{1,0:T(8,128)(2,1)} %bitcast.7, bf16[4096,256]{1,0:T(8,128)(2,1)} %bitcast.8, bf16[256,4096]{1,0:T(8,128)(2,1)} %bitcast.9, f32[1,512]{1,0:T(1,128)} %bitcast.12, ...), custom_call_target="tpu_custom_call" | custom-call | tf_op jit(solution)/shard_map/pallas_call | solution.py:533
  142.1 1.7 %copy.10 = bf16[256,512]{1,0:T(8,128)(2,1)} copy(bf16[256,512]{1,0:T(8,128)(2,1)} %shard_map.82) | data formatting | bytes 524288
